TPU v7x, 32 devices: a whole 2x2x4 slice. The times are simulated.
32 devices in a mesh: sp: 4 (over y, x), tp: 8 (over z, core).
Axes of the slice: x: 2, y: 2, z: 4, core: 2. Of those that a mesh axis runs over, the one named last changes fastest.
Arguments:
- queries: bfloat16 [2048, 1536], P('sp', 'tp'), may hold values from -34 to 34
- latent: bfloat16 [2048, 512], P('sp'), may hold values from -6 to 6
- rot_key: bfloat16 [2048, 32], P('sp'), may hold values from -34 to 34
- latent_gain: float32 [512], replicated, may hold values from 0.1 to 1.9
- key_up: bfloat16 [512, 1024], P(None, 'tp'), may hold values from -0.25 to 0.25
- value_up: bfloat16 [512, 1024], P(None, 'tp'), may hold values from -0.70710678 to 0.70710678
- query_gain: float32 [96], replicated, may hold values from 0.5 to 6
- key_gain: float32 [96], replicated, may hold values from 0.5 to 6
- out_gain: float32 [1024], replicated, may hold values from 0.1 to 1.9
- out_weight: bfloat16 [1024, 2048], replicated, may hold values from -0.1875 to 0.1875
- residual: bfloat16 [2048, 2048], P(('sp', 'tp')), may hold values from -6 to 6
- ffn_gain: float32 [2048], replicated, may hold values from 0.1 to 1.9
- routes: int32 [2048, 2], P(('sp', 'tp')), may hold values from 0 to 3, all different within a row; in each aligned block of 64 rows (0 to 63, 64 to 127, ...) at most 36 rows name the same one
- route_weights: float32 [2048, 2], P(('sp', 'tp')), may hold values from 0.2 to 1
- expert_gate: bfloat16 [4, 2048, 2048], P('sp', None, 'tp'), may hold values from -0.125 to 0.125
- expert_up: bfloat16 [4, 2048, 2048], P('sp', None, 'tp'), may hold values from -0.125 to 0.125
- expert_down: bfloat16 [4, 2048, 2048], P('sp', 'tp'), may hold values from -0.125 to 0.125
Outputs:
- layer_out: bfloat16 [2048, 2048], P(('sp', 'tp'))
Inputs may be any that keep to these rules, and one draw needn't show every extreme that they name: `routes`: the 2 experts of a token differ. Among the 64 rows of one device each expert is named by at most 36 rows, a bound that some block reaches.
All inputs are finite; a program needn't handle non-finite values.
Results may differ from a plain program's by a relative error of at most 0.02.
The roundings to bfloat16 on the way count: a program that leaves them out, or rounds other values in their place, can miss the bound.
Values may be sent and summed in bfloat16 or wider, within the bound.
No kernel may reach another device: no remote copies, remote signals or barrier semaphores. Data moves between devices by JAX's collectives and lax.ppermute only.
A program may use at most 128 MiB of HBM per device.

v0:
```python
import jax
import jax.numpy as jnp
from jax import lax
from jax.sharding import PartitionSpec as P

D = 2048
NOPE = 64
ROPE = 32
VH = 64
TOPK = 2
QK = 96
epsilon = 1e-06
rope_base = 10000.0


def rms_scale(values):
    return lax.rsqrt(jnp.mean(values * values, axis=-1, keepdims=True) + epsilon)


def rotate_half(values, angles):
    half_dims = values.shape[-1] // 2
    first_half = values[..., :half_dims]
    second_half = values[..., half_dims:]
    cosine = jnp.cos(angles)
    sine_val = jnp.sin(angles)
    return jnp.concatenate(
        [
            first_half * cosine - second_half * sine_val,
            second_half * cosine + first_half * sine_val,
        ],
        axis=-1,
    )


def head_prepare(raw_rows, gain_vec, angles):
    normed_rows = raw_rows * rms_scale(raw_rows) * gain_vec
    turned_rows = rotate_half(normed_rows[..., NOPE:], angles[:, None, :])
    return jnp.concatenate([normed_rows[..., :NOPE], turned_rows], axis=-1).astype(jnp.bfloat16)


def slot_targets(route_rows, expert_total, slot_cap):
    flat_routes = route_rows.reshape(-1)
    one_hot = (flat_routes[:, None] == jnp.arange(expert_total, dtype=jnp.int32)[None, :]).astype(
        jnp.int32
    )
    earlier = jnp.cumsum(one_hot, axis=0) - one_hot
    rank_in = jnp.sum(earlier * one_hot, axis=1)
    return (flat_routes * slot_cap + rank_in).reshape(route_rows.shape)


def select_matrix(targets, slot_total):
    hits = targets[:, :, None] == jnp.arange(slot_total, dtype=jnp.int32)[None, None, :]
    return jnp.sum(hits.astype(jnp.bfloat16), axis=1)


def shards(
    queries,
    latent,
    rot_key,
    latent_gain,
    key_up,
    value_up,
    query_gain,
    key_gain,
    out_gain,
    out_weight,
    residual,
    ffn_gain,
    routes,
    route_weights,
    expert_gate,
    expert_up,
    expert_down,
):
    shard_len = queries.shape[0]
    local_heads = key_up.shape[1] // NOPE
    sp_count = lax.axis_size("sp")
    tp_count = lax.axis_size("tp")
    my_first = lax.axis_index("sp") * shard_len
    my_last = my_first + shard_len - 1
    positions = my_first + jnp.arange(shard_len, dtype=jnp.int32)
    inverse = rope_base ** (-jnp.arange(0, ROPE, 2, dtype=jnp.float32) / ROPE)
    angles = positions.astype(jnp.float32)[:, None] * inverse[None, :]
    lat_f32 = latent.astype(jnp.float32)
    normed_latent = (lat_f32 * rms_scale(lat_f32) * latent_gain).astype(jnp.bfloat16)
    key_nope = jnp.dot(normed_latent, key_up, preferred_element_type=jnp.float32).astype(
        jnp.bfloat16
    )
    value_rows = jnp.dot(normed_latent, value_up, preferred_element_type=jnp.float32).astype(
        jnp.bfloat16
    )
    shared = jnp.broadcast_to(
        rot_key.astype(jnp.float32)[:, None, :], (shard_len, local_heads, ROPE)
    )
    raw_keys = jnp.concatenate(
        [key_nope.astype(jnp.float32).reshape(shard_len, local_heads, NOPE), shared], axis=-1
    )
    key_rows = head_prepare(raw_keys, key_gain, angles)
    query_rows = head_prepare(
        queries.astype(jnp.float32).reshape(shard_len, local_heads, QK), query_gain, angles
    )
    query_heads = jnp.transpose(query_rows, (1, 0, 2))
    bundle = jnp.concatenate(
        [
            jnp.transpose(key_rows, (1, 2, 0)),
            jnp.transpose(value_rows.reshape(shard_len, local_heads, VH), (1, 2, 0)),
        ],
        axis=1,
    )
    score_scale = QK ** (-0.5)
    init_state = (
        jnp.full((local_heads, shard_len), -1e30, jnp.float32),
        jnp.zeros((local_heads, shard_len), jnp.float32),
        jnp.zeros((local_heads, shard_len, VH), jnp.float32),
    )
    key_piece = lax.all_gather(bundle, "sp", axis=2, tiled=True)
    block_count = key_piece.shape[2] // shard_len

    def one_block(block_index, running_state):
        first_key = block_index * shard_len

        def compute(inner):
            row_peak, row_total, weighted = inner
            key_part = lax.dynamic_slice_in_dim(key_piece, block_index * shard_len, shard_len, 2)
            scores = (
                jnp.einsum(
                    "hqc,hck->hqk",
                    query_heads,
                    key_part[:, :QK, :],
                    preferred_element_type=jnp.float32,
                )
                * score_scale
            )
            key_pos = first_key + jnp.arange(shard_len, dtype=jnp.int32)
            allowed = key_pos[None, None, :] <= positions[None, :, None]
            scores = jnp.where(allowed, scores, -1e30)
            new_peak = jnp.maximum(row_peak, jnp.max(scores, axis=2))
            exponent = jnp.where(allowed, jnp.exp(scores - new_peak[..., None]), 0.0)
            factor = jnp.exp(row_peak - new_peak)
            new_total = row_total * factor + jnp.sum(exponent, axis=2)
            contrib = jnp.einsum(
                "hqk,hvk->hqv",
                exponent.astype(jnp.bfloat16),
                key_part[:, QK:, :],
                preferred_element_type=jnp.float32,
            )
            return (new_peak, new_total, weighted * factor[..., None] + contrib)

        return lax.cond(first_key <= my_last, compute, lambda inner: inner, running_state)

    row_peak, row_total, weighted = lax.fori_loop(0, block_count, one_block, init_state)
    attended = (weighted / row_total[..., None]).astype(jnp.bfloat16)
    tok_count = residual.shape[0]
    head_major = jnp.transpose(attended, (1, 0, 2)).reshape(shard_len, local_heads * VH)
    token_rows = lax.all_to_all(head_major, "tp", split_axis=0, concat_axis=1, tiled=True).astype(
        jnp.float32
    )
    normed_rows = (token_rows * rms_scale(token_rows) * out_gain).astype(jnp.bfloat16)
    partials = jnp.einsum(
        "tgc,gcd->tgd",
        normed_rows.reshape(tok_count, tp_count, -1),
        out_weight.reshape(tp_count, -1, D),
        preferred_element_type=jnp.float32,
    )
    rounded = lax.optimization_barrier(partials.astype(jnp.bfloat16))
    mixed = jnp.sum(rounded.astype(jnp.float32), axis=1)
    middle = residual.astype(jnp.float32) + mixed
    ffn_input = (middle * rms_scale(middle) * ffn_gain).astype(jnp.bfloat16)
    slot_cap = max(2, 9 * tok_count * TOPK // (8 * sp_count))
    slot_total = sp_count * slot_cap
    targets = slot_targets(routes, sp_count, slot_cap)
    chooser = select_matrix(targets, slot_total)
    outbound = (
        jnp.einsum("ts,td->sd", chooser, ffn_input, preferred_element_type=jnp.float32)
        .astype(jnp.bfloat16)
        .reshape(sp_count, slot_cap, D)
    )
    arrived = lax.all_to_all(outbound, "sp", split_axis=0, concat_axis=0, tiled=True)
    item_count = arrived.shape[1]
    flat_rows = arrived.reshape(sp_count * item_count, D)
    row_block = lax.all_gather(flat_rows, "tp", axis=0, tiled=True)
    gate_pre = jnp.dot(row_block, expert_gate[0], preferred_element_type=jnp.float32)
    up_pre = jnp.dot(row_block, expert_up[0], preferred_element_type=jnp.float32)
    hidden = (jax.nn.silu(gate_pre) * up_pre).astype(jnp.bfloat16)
    served = lax.psum_scatter(
        jnp.dot(hidden, expert_down[0], preferred_element_type=jnp.float32).astype(jnp.bfloat16),
        "tp",
        scatter_dimension=0,
        tiled=True,
    ).reshape(sp_count, item_count, D)
    returned_rows = lax.all_to_all(served, "sp", split_axis=0, concat_axis=0, tiled=True).reshape(
        slot_total, D
    )
    picked = (
        jnp.take(returned_rows, targets.reshape(-1), axis=0)
        .reshape(tok_count, TOPK, D)
        .astype(jnp.float32)
    )
    moe_sum = jnp.sum(picked * route_weights[:, :, None], axis=1)
    return (middle + moe_sum).astype(jnp.bfloat16)


def solution(mesh):
    return jax.shard_map(
        shards,
        mesh=mesh,
        in_specs=(
            P("sp", "tp"),
            P("sp", None),
            P("sp", None),
            P(),
            P(None, "tp"),
            P(None, "tp"),
            P(),
            P(),
            P(),
            P(),
            P(("sp", "tp"), None),
            P(),
            P(("sp", "tp"), None),
            P(("sp", "tp"), None),
            P("sp", None, "tp"),
            P("sp", None, "tp"),
            P("sp", "tp", None),
        ),
        out_specs=P(("sp", "tp"), None),
        check_vma=False,
    )
```

profile of v0, /device:TPU:0, one launch (start us, length us, event | category | flops | bytes accessed | tf_op | source)
XLA Modules:
  0.0 237.7 jit_solution(2543511276037347893)
XLA Ops:
  6.6 1.3 fusion.25
  8.0 1.5 bitcast_convert_fusion
  9.5 0.8 broadcast_in_dim.40
  10.5 0.1 fusion.35
  10.6 0.4 convolution_convert_fusion.3
  11.1 0.2 multiply_cosine_fusion
  11.3 0.8 pad_maximum_fusion.1
  12.3 0.1 reshape.250
  12.5 0.2 reduce_window_sum.11
  12.7 0.2 select_reduce_fusion
  12.9 0.1 reduce_sum.103
  13.1 0.7 maximum_bitcast_fusion.1
  13.8 29.8 %all-gather.3.cloned.1.call-done = bf16[2,160,2048]{2,1,0:T(8,128)(2,1)} async-done(((bf16[2,160,512]{2,1,0:T(8,128)(2,1)}), bf16[2,160,2048]{2,1,0:T(8,128)(2,1)}) %all-gather.3.cloned.1.call-update) | async-done | bytes 1310736 | tf_op jit(solution)/shard_map/all_gather | solution.py:116
  43.6 0.7 broadcast_in_dim.39
  44.3 5.1 %while.18 = (s32[]{:T(128)}, f32[2,512]{1,0:T(2,128)S(1)}, f32[2,512]{1,0:T(2,128)S(1)}, f32[2,512,64]{1,2,0:T(8,128)}, s32[]{:T(128)}, /*index=5*/bf16[2,160,20...) while((s32[]{:T(128)}, f32[2,512]{1,0:T(2,128)S(1)}, ...), condition=%wide.region_8.9_spmd.clone, body=%wide.region_3.8_spmd.clone.sunk | while | flops 174984192 | bytes 8466765 | solution.py:151
  44.3 5.0 %conditional.3 = ((f32[2,512]{1,0:T(2,128)S(1)}, f32[2,512]{1,0:T(2,128)S(1)}, f32[2,512,64]{1,2,0:T(8,128)})) conditional(s32[]{:T(128)} %convert_element_type.181, (f32[2,512]{1,0:T(2,128)S(1)}, f32[2,512]{1,0:T(2,128)S(1)}, f32[2,512,64]{1,2,0:T(8,128)}) %tuple.52, (s32[]{:T(128)}, s32[]{:T(128)}, s32[]{:T(128)}, bf16[2,160,2048]{2,1,0:T(8,128)(2,1)}, ...), branch_computations={%region_4.0_spmd, %region_5.7_spmd} | conditional | flops 174984192 | bytes 8464494 | solution.py:149
  44.3 0.2 broadcast_compare_fusion
  44.6 1.7 fusion.2
  46.3 0.6 fusion.4
  46.8 2.5 %convolution_add_fusion = f32[2,512,64]{1,2,0:T(8,128)} fusion(f32[2,512,512]{2,1,0:T(8,128)S(1)} %get-tuple-element.232, f32[2,512]{1,0:T(2,128)S(1)} %max.2, pred[512,512]{0,1:T(8,128)(4,1)S(1)} %broadcast_compare_fusion, f32[2,512,64]{1,2,0:T(8,128)} %get-tuple-element.169, bf16[2,160,2048]{2,1,0:T(8,128)(2,1)} %get-tuple-element.165, s32[]{:T(128)S(6)} %add.179, ...), kind=kOutput, calls=%fused_computation.7 | convolution fusion | flops 69861376 | bytes 3022856 | tf_op jit(solution)/shard_map/while/body/eval_jaxpr/cond/branch_1_fun/hqk,hvk->hqv/dot_general | solution.py:141
  49.4 1.0 fusion.47
  50.4 0.2 all_to_all.16
  50.6 0.8 copy.46
  51.5 4.6 %all-to-all-start = ((bf16[8,64,128]{2,1,0:T(8,128)(2,1)}), bf16[8,64,128]{2,1,0:T(8,128)(2,1)S(1)}, u32[]{:S(2)}, u32[]{:S(2)}) async-start(bf16[8,64,128]{2,1,0:T(8,128)(2,1)} %copy.46), calls=%async_computation | async-start | bytes 262144 | tf_op jit(solution)/shard_map/all_to_all | solution.py:155
  56.2 6.6 %all-to-all-done = bf16[8,64,128]{2,1,0:T(8,128)(2,1)S(1)} async-done(((bf16[8,64,128]{2,1,0:T(8,128)(2,1)}), bf16[8,64,128]{2,1,0:T(8,128)(2,1)S(1)}, u32[]{:S(2)}, u32[]{:S(2)}) %all-to-all-start) | async-done | bytes 131104 | tf_op jit(solution)/shard_map/all_to_all | solution.py:155
  62.8 0.1 fusion.36
  62.9 3.0 %fusion.18 = bf16[64,8,2048]{2,0,1:T(8,128)(2,1)S(1)} fusion(bf16[8,128,2048]{2,1,0:T(8,128)(2,1)} %bitcast.57, bf16[8,64,128]{2,1,0:T(8,128)(2,1)S(1)} %all-to-all-done, f32[8,128]{1,0:T(8,128)S(1)} %bitcast.61, f32[64]{0:T(128)S(1)} %add_rsqrt_fusion.4), kind=kOutput, calls=%fused_computation.29 | convolution fusion | flops 269746176 | bytes 6426880 | tf_op jit(solution)/shard_map/tgc,gcd->tgd/dot_general | solution.py:159
  65.9 0.4 convert_reduce_fusion
  66.3 0.6 copy-done.1
  66.9 0.2 multiply_reduce_fusion.1
  67.1 0.4 convolution_convert_fusion.2
  67.4 0.1 reshape.251
  67.6 27.1 %all_to_all.23 = bf16[4,36,2048]{2,1,0:T(8,128)(2,1)S(1)} all-to-all(bf16[4,36,2048]{2,1,0:T(8,128)(2,1)S(1)} %reshape.251), channel_id=1, replica_groups=mesh['sp'=4,'tp'=8] {'sp'}, dimensions={0} | all-to-all | bytes 1179648 | tf_op jit(solution)/shard_map/all_to_all | solution.py:178
  94.7 1.0 reshape.252
  95.7 0.2 reduce-scatter.2.cloned.1.call-start
  95.9 48.8 %all-gather.5.cloned.1.call-done = bf16[1152,2048]{1,0:T(8,128)(2,1)} async-done(((bf16[144,2048]{1,0:T(8,128)(2,1)}), bf16[1152,2048]{1,0:T(8,128)(2,1)}) %all-gather.5.cloned.1.call-update) | async-done | bytes 4718608 | tf_op jit(solution)/shard_map/all_gather | solution.py:181
  144.7 5.0 %fusion.31 = f32[1152,256]{1,0:T(8,128)} fusion(bf16[1152,2048]{1,0:T(8,128)(2,1)} %all-gather.5.cloned.1.call-done, bf16[1,2048,256]{2,1,0:T(8,128)(2,1)} %param.35), kind=kOutput, calls=%fused_computation.46 | convolution fusion | flops 1207959552 | bytes 6946816 | tf_op jit(solution)/shard_map/dot_general | solution.py:182
  149.7 9.7 %convolution_convert_fusion = bf16[1152,2048]{1,0:T(8,128)(2,1)} fusion(bf16[1152,2048]{1,0:T(8,128)(2,1)} %all-gather.5.cloned.1.call-done, f32[1152,256]{1,0:T(8,128)} %fusion.31, bf16[1,256,2048]{2,1,0:T(8,128)(2,1)S(1)} %copy-done, bf16[1,2048,256]{2,1,0:T(8,128)(2,1)S(1)} %copy-done.10), kind=kOutput, calls=%fused_computation.25 | convolution fusion | flops 2420047872 | bytes 12713984 | tf_op jit(solution)/shard_map/dot_general | solution.py:186
  159.5 53.8 %reduce-scatter.2.cloned.1.call-done = bf16[144,2048]{1,0:T(8,128)(2,1)} async-done(((bf16[1152,2048]{1,0:T(8,128)(2,1)}), bf16[144,2048]{1,0:T(8,128)(2,1)}) %reduce-scatter.2.cloned.1.call-update) | async-done | bytes 589840 | tf_op jit(solution)/shard_map/reduce_scatter | solution.py:185
  213.3 2.0 reshape.253
  215.3 3.6 %all-to-all-start.2 = ((bf16[4,36,2048]{2,1,0:T(8,128)(2,1)}), bf16[4,36,2048]{2,1,0:T(8,128)(2,1)S(1)}, u32[]{:S(2)}, u32[]{:S(2)}) async-start(bf16[4,36,2048]{2,1,0:T(8,128)(2,1)} %reshape.253), calls=%async_computation.3 | async-start | bytes 1310720 | tf_op jit(solution)/shard_map/all_to_all | solution.py:191
  219.0 0.1 mul.297
  219.4 7.2 %all-to-all-done.2 = bf16[4,36,2048]{2,1,0:T(8,128)(2,1)S(1)} async-done(((bf16[4,36,2048]{2,1,0:T(8,128)(2,1)}), bf16[4,36,2048]{2,1,0:T(8,128)(2,1)S(1)}, u32[]{:S(2)}, u32[]{:S(2)}) %all-to-all-start.2) | async-done | bytes 589856 | tf_op jit(solution)/shard_map/all_to_all | solution.py:191
  226.6 0.1 reshape.254
  226.7 0.9 gather_fusion
  227.7 0.3 gather.7
  228.0 2.3 multiply_reduce_fusion
  230.4 0.8 add_convert_fusion
  (67 shorter events, 1.2 us)
Async XLA Ops:
  6.5 143.2 %copy-start = (bf16[1,256,2048]{2,1,0:T(8,128)(2,1)S(1)}, bf16[1,256,2048]{2,1,0:T(8,128)(2,1)}, u32[]{:S(2)}) copy-start(bf16[1,256,2048]{2,1,0:T(8,128)(2,1)} %param.37) | copy-start | bytes 3145732
  6.5 4.1 %copy-start.3 = (bf16[512,512]{1,0:T(8,128)(2,1)S(1)}, bf16[512,512]{1,0:T(8,128)(2,1)}, u32[]{:S(2)}) copy-start(bf16[512,512]{1,0:T(8,128)(2,1)} %param.22) | copy-start | bytes 1572868
  6.5 4.1 %copy-start.12 = (f32[512]{0:T(512)S(1)}, f32[512]{0:T(512)}, u32[]{:S(2)}) copy-start(f32[512]{0:T(512)} %param.24) | copy-start | bytes 6148
  6.5 3.8 %copy-start.2 = (bf16[512,192]{0,1:T(8,128)(2,1)S(1)}, bf16[512,192]{0,1:T(8,128)(2,1)}, u32[]{:S(2)}) copy-start(bf16[512,192]{0,1:T(8,128)(2,1)} %param.21) | copy-start | bytes 589828
  6.5 3.9 %copy-start.8 = (f32[96]{0:T(128)S(1)}, f32[96]{0:T(128)}, u32[]{:S(2)}) copy-start(f32[96]{0:T(128)} %param.27) | copy-start | bytes 1156
  6.5 3.9 %copy-start.9 = (f32[96]{0:T(128)S(1)}, f32[96]{0:T(128)}, u32[]{:S(2)}) copy-start(f32[96]{0:T(128)} %param.28) | copy-start | bytes 1156
  6.6 4.1 %copy-start.11 = (bf16[512,128]{1,0:T(8,128)(2,1)S(1)}, bf16[512,128]{1,0:T(8,128)(2,1)}, u32[]{:S(2)}) copy-start(bf16[512,128]{1,0:T(8,128)(2,1)} %param.26) | copy-start | bytes 393220
  6.6 37.0 %all-gather.3.cloned.1.call-start = ((), (), s32[]{:S(2)}) async-start(), calls=%async_computation.4 | async-start | bytes 1638400 | tf_op jit(solution)/shard_map/all_gather | solution.py:116
  10.5 1.7 copy-start.4
  44.3 18.6 %copy-start.6 = (f32[1024]{0:T(1024)S(1)}, f32[1024]{0:T(1024)}, u32[]{:S(2)}) copy-start(f32[1024]{0:T(1024)} %param.29) | copy-start | bytes 12292
  51.5 11.3 %all-to-all-start = ((bf16[8,64,128]{2,1,0:T(8,128)(2,1)}), bf16[8,64,128]{2,1,0:T(8,128)(2,1)S(1)}, u32[]{:S(2)}, u32[]{:S(2)}) async-start(bf16[8,64,128]{2,1,0:T(8,128)(2,1)} %copy.46), calls=%async_computation | async-start | bytes 262144 | tf_op jit(solution)/shard_map/all_to_all | solution.py:155
  56.1 88.6 %all-gather.5.cloned.1.call-start = ((), (), s32[]{:S(2)}) async-start(), calls=%async_computation.5 | async-start | bytes 5308416 | tf_op jit(solution)/shard_map/all_gather | solution.py:181
  65.9 1.0 copy-start.1
  65.9 1.1 copy-start.5
  95.6 54.1 %copy-start.10 = (bf16[1,2048,256]{2,1,0:T(8,128)(2,1)S(1)}, bf16[1,2048,256]{2,1,0:T(8,128)(2,1)}, u32[]{:S(2)}) copy-start(bf16[1,2048,256]{2,1,0:T(8,128)(2,1)} %param.36) | copy-start | bytes 3145732
  95.7 117.6 %reduce-scatter.2.cloned.1.call-start = ((), (), s32[]{:S(2)}) async-start(), calls=%async_computation.6 | async-start | bytes 5308416 | tf_op jit(solution)/shard_map/reduce_scatter | solution.py:185
  159.5 59.8 %copy-start.7 = (f32[64,2]{0,1:T(2,128)S(1)}, f32[64,2]{0,1:T(2,128)}, u32[]{:S(2)}) copy-start(f32[64,2]{0,1:T(2,128)} %param.34) | copy-start | bytes 1540
  215.3 11.3 %all-to-all-start.2 = ((bf16[4,36,2048]{2,1,0:T(8,128)(2,1)}), bf16[4,36,2048]{2,1,0:T(8,128)(2,1)S(1)}, u32[]{:S(2)}, u32[]{:S(2)}) async-start(bf16[4,36,2048]{2,1,0:T(8,128)(2,1)} %reshape.253), calls=%async_computation.3 | async-start | bytes 1310720 | tf_op jit(solution)/shard_map/all_to_all | solution.py:191
Sparse Core Ops, SparseCore 0:
  12.3 31.2 all-gather.2
  95.8 48.8 all-gather.4
  159.6 53.6 reduce-scatter.1
where the time goes:
time: 238 us
  waiting for transfers between devices  146 us (61%)
  blocking collectives  27.1 us (11%)
  matrix products  24.2 us (10%)
  between operations  13.5 us (6%)
  other arithmetic  9.45 us (4%)
  local copies, waits for them, and re-layouts  8.58 us (4%)
  starting transfers between devices  8.54 us (4%)
    reduce_scatter x1, waiting for transfers between devices, shards(): lax.psum_scatter(jnp.dot(hidden, expert_down[0], preferred_element_type=j...  53.8 us
    all_gather x1, waiting for transfers between devices, shards(): row_block = lax.all_gather(flat_rows, 'tp', axis=0, tiled=True)  48.8 us
    all_gather x1, waiting for transfers between devices, shards(): key_piece = lax.all_gather(bundle, 'sp', axis=2, tiled=True)  29.8 us
    all_to_all x1, blocking collectives, shards(): lax.all_to_all(outbound, 'sp', split_axis=0, concat_axis=0, tiled=True)  27.1 us
    dot_general x1, matrix products, shards(): jnp.dot(hidden, expert_down[0], preferred_element_type=jnp.float32)  9.73 us
    all_to_all x1, waiting for transfers between devices, shards(): lax.all_to_all(served, 'sp', split_axis=0, concat_axis=0, tiled=True)  7.23 us
    all_to_all x1, waiting for transfers between devices, shards(): lax.all_to_all(head_major, 'tp', split_axis=0, concat_axis=1, tiled=True)  6.6 us
    dot_general x1, matrix products, shards(): jnp.dot(row_block, expert_gate[0], preferred_element_type=jnp.float32)  5.04 us
  transfers between devices with their start and end apart: 5, of which 5 were waited for; matrix products, arithmetic and copies ran while one was open for 1% of the time, Pallas kernels for 0%

commit v1 on v0

--- a/solution.py
+++ b/solution.py
@@ -11,6 +11,22 @@
 QK = 96
 epsilon = 1e-06
 rope_base = 10000.0
+
+
+def swapped_with_each(shard, axis, split, join):
+    ways, here = (lax.axis_size(axis), lax.axis_index(axis))
+    width = shard.shape[split] // ways
+    lengths = list(shard.shape)
+    lengths[split] = width
+    height = lengths[join]
+    lengths[join] = height * ways
+    full = jnp.zeros(lengths, shard.dtype)
+    for mask in range(ways):
+        part = lax.dynamic_slice_in_dim(shard, (here ^ mask) * width, width, axis=split)
+        if mask:
+            part = lax.ppermute(part, axis, [(d, d ^ mask) for d in range(ways)])
+        full = lax.dynamic_update_slice_in_dim(full, part, (here ^ mask) * height, axis=join)
+    return full
 
 
 def rms_scale(values):
@@ -152,9 +168,7 @@
     attended = (weighted / row_total[..., None]).astype(jnp.bfloat16)
     tok_count = residual.shape[0]
     head_major = jnp.transpose(attended, (1, 0, 2)).reshape(shard_len, local_heads * VH)
-    token_rows = lax.all_to_all(head_major, "tp", split_axis=0, concat_axis=1, tiled=True).astype(
-        jnp.float32
-    )
+    token_rows = swapped_with_each(head_major, "tp", 0, 1).astype(jnp.float32)
     normed_rows = (token_rows * rms_scale(token_rows) * out_gain).astype(jnp.bfloat16)
     partials = jnp.einsum(
         "tgc,gcd->tgd",

time: 238 us -> 240 us (level)
  starting transfers between devices: 8.54 us -> 12.4 us
  waiting for transfers between devices: 146 us -> 143 us
    ppermute x0 -> x7, starting transfers between devices: none -> 8.5 us  [swapped_with_each(): part = lax.ppermute(part, axis, [(d, d ^ mask) for d in range(ways)])]
    all_to_all x1 -> x0, waiting for transfers between devices: 6.6 us -> none  [shards(): lax.all_to_all(head_major, 'tp', split_axis=0, concat_axis=1, tiled=True)]
    all_to_all x1 -> x0, starting transfers between devices: 4.6 us -> none  [shards(): lax.all_to_all(head_major, 'tp', split_axis=0, concat_axis=1, tiled=True)]
    ppermute x0 -> x7, waiting for transfers between devices: none -> 4.56 us  [swapped_with_each(): part = lax.ppermute(part, axis, [(d, d ^ mask) for d in range(ways)])]
  transfers between devices with their start and end apart: 5 -> 11, of which waited for: 5 -> 6; matrix products, arithmetic and copies ran while one was open for 1% -> 1% of each run, Pallas kernels for 0% -> 0%
where the time goes in v1:
time: 240 us; the launch traced here: 239 us
  waiting for transfers between devices  143 us (60%)
  blocking collectives  27.8 us (12%)
  matrix products  24.2 us (10%)
  between operations  13.7 us (6%)
  starting transfers between devices  12.4 us (5%)
  other arithmetic  9.44 us (4%)
  local copies, waits for them, and re-layouts  8.5 us (4%)
    reduce_scatter x1, waiting for transfers between devices, shards(): lax.psum_scatter(jnp.dot(hidden, expert_down[0], preferred_element_type=j...  53.8 us
    all_gather x1, waiting for transfers between devices, shards(): row_block = lax.all_gather(flat_rows, 'tp', axis=0, tiled=True)  47.8 us
    all_gather x1, waiting for transfers between devices, shards(): key_piece = lax.all_gather(bundle, 'sp', axis=2, tiled=True)  29.5 us
    all_to_all x1, blocking collectives, shards(): lax.all_to_all(outbound, 'sp', split_axis=0, concat_axis=0, tiled=True)  27.8 us
    dot_general x1, matrix products, shards(): jnp.dot(hidden, expert_down[0], preferred_element_type=jnp.float32)  9.72 us
    ppermute x7, starting transfers between devices, swapped_with_each(): part = lax.ppermute(part, axis, [(d, d ^ mask) for d in range(ways)])  8.5 us
    all_to_all x1, waiting for transfers between devices, shards(): lax.all_to_all(served, 'sp', split_axis=0, concat_axis=0, tiled=True)  7.2 us
    dot_general x1, matrix products, shards(): jnp.dot(row_block, expert_gate[0], preferred_element_type=jnp.float32)  5.04 us
  transfers between devices with their start and end apart: 11, of which 6 were waited for; matrix products, arithmetic and copies ran while one was open for 1% of the time, Pallas kernels for 0%

profile of v1, /device:TPU:0, one launch (start us, length us, event | category | flops | bytes accessed | tf_op | source)
XLA Modules:
  0.0 239.1 jit_solution(7476746043038087122)
XLA Ops:
  6.6 1.3 fusion.25
  8.0 1.5 bitcast_convert_fusion
  9.5 0.8 broadcast_in_dim.43
  10.6 0.4 convolution_convert_fusion.3
  11.1 0.2 multiply_cosine_fusion
  11.3 0.8 pad_maximum_fusion.1
  12.4 0.1 reshape.242
  12.6 0.2 reduce_window_sum.11
  12.8 0.2 select_reduce_fusion
  13.0 0.1 reduce_sum.103
  13.3 0.7 maximum_bitcast_fusion.1
  14.0 29.5 %all-gather.3.cloned.1.call-done = bf16[2,160,2048]{2,1,0:T(8,128)(2,1)} async-done(((bf16[2,160,512]{2,1,0:T(8,128)(2,1)}), bf16[2,160,2048]{2,1,0:T(8,128)(2,1)}) %all-gather.3.cloned.1.call-update) | async-done | bytes 1310736 | tf_op jit(solution)/shard_map/all_gather | solution.py:132
  43.6 0.7 broadcast_in_dim.42
  44.3 5.1 %while.18 = (s32[]{:T(128)}, f32[2,512]{1,0:T(2,128)S(1)}, f32[2,512]{1,0:T(2,128)S(1)}, f32[2,512,64]{1,2,0:T(8,128)}, s32[]{:T(128)}, /*index=5*/bf16[2,160,20...) while((s32[]{:T(128)}, f32[2,512]{1,0:T(2,128)S(1)}, ...), condition=%wide.region_8.9_spmd.clone, body=%wide.region_3.8_spmd.clone.sunk | while | flops 174984192 | bytes 8466765 | solution.py:167
  44.3 5.0 %conditional.3 = ((f32[2,512]{1,0:T(2,128)S(1)}, f32[2,512]{1,0:T(2,128)S(1)}, f32[2,512,64]{1,2,0:T(8,128)})) conditional(s32[]{:T(128)} %convert_element_type.173, (f32[2,512]{1,0:T(2,128)S(1)}, f32[2,512]{1,0:T(2,128)S(1)}, f32[2,512,64]{1,2,0:T(8,128)}) %tuple.59, (s32[]{:T(128)}, s32[]{:T(128)}, s32[]{:T(128)}, bf16[2,160,2048]{2,1,0:T(8,128)(2,1)}, ...), branch_computations={%region_4.0_spmd, %region_5.7_spmd} | conditional | flops 174984192 | bytes 8464494 | solution.py:165
  44.3 0.2 broadcast_compare_fusion
  44.6 1.7 fusion.2
  46.2 0.6 fusion.4
  46.8 2.5 %convolution_add_fusion = f32[2,512,64]{1,2,0:T(8,128)} fusion(f32[2,512,512]{2,1,0:T(8,128)S(1)} %get-tuple-element.232, f32[2,512]{1,0:T(2,128)S(1)} %max.2, pred[512,512]{0,1:T(8,128)(4,1)S(1)} %broadcast_compare_fusion, f32[2,512,64]{1,2,0:T(8,128)} %get-tuple-element.169, bf16[2,160,2048]{2,1,0:T(8,128)(2,1)} %get-tuple-element.165, s32[]{:T(128)S(6)} %add.243, ...), kind=kOutput, calls=%fused_computation.7 | convolution fusion | flops 69861376 | bytes 3022856 | tf_op jit(solution)/shard_map/while/body/eval_jaxpr/cond/branch_1_fun/hqk,hvk->hqv/dot_general | solution.py:157
  49.4 1.0 divide_convert_fusion
  50.4 0.2 constant_dynamic-slice_fusion
  51.0 1.5 collective-permute-start.1
  52.6 0.4 collective-permute-start.2
  53.1 2.5 %collective-permute-start.3 = (bf16[64,128]{1,0:T(8,128)(2,1)S(1)}, bf16[64,128]{1,0:T(8,128)(2,1)S(1)}, u32[]{:S(2)}, u32[]{:S(2)}) collective-permute-start(bf16[64,128]{1,0:T(8,128)(2,1)S(1)} %copy.69), channel_id=1, source_target_pairs={{0,4},{1,5},{2,6},{3,7},{4,0},{5,1},{6,2},{7,3},{8,12},{9,13},{10,... | collective-permute-start | bytes 49160 | tf_op jit(solution)/shard_map/ppermute | solution.py:27
  55.7 0.2 collective-permute-start.4
  56.1 3.4 %collective-permute-start.5 = (bf16[64,128]{1,0:T(8,128)(2,1)S(1)}, bf16[64,128]{1,0:T(8,128)(2,1)S(1)}, u32[]{:S(2)}, u32[]{:S(2)}) collective-permute-start(bf16[64,128]{1,0:T(8,128)(2,1)S(1)} %copy.71), channel_id=1, source_target_pairs={{0,6},{1,7},{2,4},{3,5},{4,2},{5,3},{6,0},{7,1},{8,14},{9,15},{10,... | collective-permute-start | bytes 49160 | tf_op jit(solution)/shard_map/ppermute | solution.py:27
  59.5 0.4 collective-permute-start.6
  60.0 1.7 collective-permute-done.5
  61.7 2.8 %collective-permute-done.6 = bf16[64,128]{1,0:T(8,128)(2,1)S(1)} collective-permute-done((bf16[64,128]{1,0:T(8,128)(2,1)S(1)}, bf16[64,128]{1,0:T(8,128)(2,1)S(1)}, u32[]{:S(2)}, u32[]{:S(2)}) %collective-permute-start.6) | collective-permute-done | bytes 16416 | tf_op jit(solution)/shard_map/ppermute | solution.py:27
  64.7 3.0 %fusion.18 = bf16[64,8,2048]{2,0,1:T(8,128)(2,1)S(1)} fusion(bf16[8,128,2048]{2,1,0:T(8,128)(2,1)} %bitcast.59, bf16[64,1024]{1,0:T(8,128)(2,1)S(1)} %constant_dynamic-update-slice_fusion, f32[1024]{0:T(1024)S(1)} %copy-done.6, f32[64]{0:T(128)S(1)} %add_rsqrt_fusion.4), kind=kOutput, calls=%fused_computation.29 | convolution fusion | flops 269746176 | bytes 6426880 | tf_op jit(solution)/shard_map/tgc,gcd->tgd/dot_general | solution.py:173
  67.7 0.4 convert_reduce_fusion
  68.1 0.6 copy-done.1
  68.6 0.2 multiply_reduce_fusion.1
  68.8 0.4 convolution_convert_fusion.2
  69.3 27.8 %all_to_all.10 = bf16[4,36,2048]{2,1,0:T(8,128)(2,1)S(1)} all-to-all(bf16[4,36,2048]{2,1,0:T(8,128)(2,1)S(1)} %reshape.243), channel_id=1, replica_groups=mesh['sp'=4,'tp'=8] {'sp'}, dimensions={0} | all-to-all | bytes 1179648 | tf_op jit(solution)/shard_map/all_to_all | solution.py:192
  97.1 0.9 reshape.244
  98.1 0.2 reduce-scatter.2.cloned.1.call-start
  98.3 47.8 %all-gather.5.cloned.1.call-done = bf16[1152,2048]{1,0:T(8,128)(2,1)} async-done(((bf16[144,2048]{1,0:T(8,128)(2,1)}), bf16[1152,2048]{1,0:T(8,128)(2,1)}) %all-gather.5.cloned.1.call-update) | async-done | bytes 4718608 | tf_op jit(solution)/shard_map/all_gather | solution.py:195
  146.1 5.0 %fusion.31 = f32[1152,256]{1,0:T(8,128)} fusion(bf16[1152,2048]{1,0:T(8,128)(2,1)} %all-gather.5.cloned.1.call-done, bf16[1,2048,256]{2,1,0:T(8,128)(2,1)} %param.35), kind=kOutput, calls=%fused_computation.46 | convolution fusion | flops 1207959552 | bytes 6946816 | tf_op jit(solution)/shard_map/dot_general | solution.py:196
  151.1 9.7 %convolution_convert_fusion = bf16[1152,2048]{1,0:T(8,128)(2,1)} fusion(bf16[1152,2048]{1,0:T(8,128)(2,1)} %all-gather.5.cloned.1.call-done, f32[1152,256]{1,0:T(8,128)} %fusion.31, bf16[1,256,2048]{2,1,0:T(8,128)(2,1)S(1)} %copy-done, bf16[1,2048,256]{2,1,0:T(8,128)(2,1)S(1)} %copy-done.10), kind=kOutput, calls=%fused_computation.25 | convolution fusion | flops 2420047872 | bytes 12713984 | tf_op jit(solution)/shard_map/dot_general | solution.py:200
  160.9 53.8 %reduce-scatter.2.cloned.1.call-done = bf16[144,2048]{1,0:T(8,128)(2,1)} async-done(((bf16[1152,2048]{1,0:T(8,128)(2,1)}), bf16[144,2048]{1,0:T(8,128)(2,1)}) %reduce-scatter.2.cloned.1.call-update) | async-done | bytes 589840 | tf_op jit(solution)/shard_map/reduce_scatter | solution.py:199
  214.7 2.0 reshape.245
  216.7 3.6 %all-to-all-start.1 = ((bf16[4,36,2048]{2,1,0:T(8,128)(2,1)}), bf16[4,36,2048]{2,1,0:T(8,128)(2,1)S(1)}, u32[]{:S(2)}, u32[]{:S(2)}) async-start(bf16[4,36,2048]{2,1,0:T(8,128)(2,1)} %reshape.245), calls=%async_computation.2 | async-start | bytes 1310720 | tf_op jit(solution)/shard_map/all_to_all | solution.py:205
  220.8 7.2 %all-to-all-done.1 = bf16[4,36,2048]{2,1,0:T(8,128)(2,1)S(1)} async-done(((bf16[4,36,2048]{2,1,0:T(8,128)(2,1)}), bf16[4,36,2048]{2,1,0:T(8,128)(2,1)S(1)}, u32[]{:S(2)}, u32[]{:S(2)}) %all-to-all-start.1) | async-done | bytes 589856 | tf_op jit(solution)/shard_map/all_to_all | solution.py:205
  228.2 0.9 gather_fusion
  229.1 0.3 gather.7
  229.4 2.3 multiply_reduce_fusion
  231.8 0.8 add_convert_fusion
  (95 shorter events, 2.7 us)
Async XLA Ops:
  6.5 144.6 %copy-start = (bf16[1,256,2048]{2,1,0:T(8,128)(2,1)S(1)}, bf16[1,256,2048]{2,1,0:T(8,128)(2,1)}, u32[]{:S(2)}) copy-start(bf16[1,256,2048]{2,1,0:T(8,128)(2,1)} %param.37) | copy-start | bytes 3145732
  6.5 4.1 %copy-start.3 = (bf16[512,512]{1,0:T(8,128)(2,1)S(1)}, bf16[512,512]{1,0:T(8,128)(2,1)}, u32[]{:S(2)}) copy-start(bf16[512,512]{1,0:T(8,128)(2,1)} %param.22) | copy-start | bytes 1572868
  6.5 4.1 %copy-start.12 = (f32[512]{0:T(512)S(1)}, f32[512]{0:T(512)}, u32[]{:S(2)}) copy-start(f32[512]{0:T(512)} %param.24) | copy-start | bytes 6148
  6.5 3.8 %copy-start.2 = (bf16[512,192]{0,1:T(8,128)(2,1)S(1)}, bf16[512,192]{0,1:T(8,128)(2,1)}, u32[]{:S(2)}) copy-start(bf16[512,192]{0,1:T(8,128)(2,1)} %param.21) | copy-start | bytes 589828
  6.5 3.9 %copy-start.8 = (f32[96]{0:T(128)S(1)}, f32[96]{0:T(128)}, u32[]{:S(2)}) copy-start(f32[96]{0:T(128)} %param.27) | copy-start | bytes 1156
  6.5 3.9 %copy-start.9 = (f32[96]{0:T(128)S(1)}, f32[96]{0:T(128)}, u32[]{:S(2)}) copy-start(f32[96]{0:T(128)} %param.28) | copy-start | bytes 1156
  6.6 4.1 %copy-start.11 = (bf16[512,128]{1,0:T(8,128)(2,1)S(1)}, bf16[512,128]{1,0:T(8,128)(2,1)}, u32[]{:S(2)}) copy-start(bf16[512,128]{1,0:T(8,128)(2,1)} %param.26) | copy-start | bytes 393220
  6.6 37.0 %all-gather.3.cloned.1.call-start = ((), (), s32[]{:S(2)}) async-start(), calls=%async_computation.3 | async-start | bytes 1638400 | tf_op jit(solution)/shard_map/all_gather | solution.py:132
  10.6 1.7 copy-start.4
  12.1 134.0 %all-gather.5.cloned.1.call-start = ((), (), s32[]{:S(2)}) async-start(), calls=%async_computation.4 | async-start | bytes 5308416 | tf_op jit(solution)/shard_map/all_gather | solution.py:195
  44.3 20.4 %copy-start.6 = (f32[1024]{0:T(1024)S(1)}, f32[1024]{0:T(1024)}, u32[]{:S(2)}) copy-start(f32[1024]{0:T(1024)} %param.29) | copy-start | bytes 12292
  50.8 5.3 %collective-permute-start = (bf16[64,128]{1,0:T(8,128)(2,1)S(1)}, bf16[64,128]{1,0:T(8,128)(2,1)S(1)}, u32[]{:S(2)}, u32[]{:S(2)}) collective-permute-start(bf16[64,128]{1,0:T(8,128)(2,1)S(1)} %copy.66), channel_id=1, source_target_pairs={{0,1},{1,0},{2,3},{3,2},{4,5},{5,4},{6,7},{7,6},{8,9},{9,8},{10,11... | collective-permute-start | bytes 49160 | tf_op jit(solution)/shard_map/ppermute | solution.py:27
  51.0 8.6 %collective-permute-start.1 = (bf16[64,128]{1,0:T(8,128)(2,1)S(1)}, bf16[64,128]{1,0:T(8,128)(2,1)S(1)}, u32[]{:S(2)}, u32[]{:S(2)}) collective-permute-start(bf16[64,128]{1,0:T(8,128)(2,1)S(1)} %copy.67), channel_id=1, source_target_pairs={{0,2},{1,3},{2,0},{3,1},{4,6},{5,7},{6,4},{7,5},{8,10},{9,11},{10,... | collective-permute-start | bytes 49160 | tf_op jit(solution)/shard_map/ppermute | solution.py:27
  52.6 7.3 %collective-permute-start.2 = (bf16[64,128]{1,0:T(8,128)(2,1)S(1)}, bf16[64,128]{1,0:T(8,128)(2,1)S(1)}, u32[]{:S(2)}, u32[]{:S(2)}) collective-permute-start(bf16[64,128]{1,0:T(8,128)(2,1)S(1)} %copy.68), channel_id=1, source_target_pairs={{0,3},{1,2},{2,1},{3,0},{4,7},{5,6},{6,5},{7,4},{8,11},{9,10},{10,... | collective-permute-start | bytes 49160 | tf_op jit(solution)/shard_map/ppermute | solution.py:27
  53.1 6.8 %collective-permute-start.3 = (bf16[64,128]{1,0:T(8,128)(2,1)S(1)}, bf16[64,128]{1,0:T(8,128)(2,1)S(1)}, u32[]{:S(2)}, u32[]{:S(2)}) collective-permute-start(bf16[64,128]{1,0:T(8,128)(2,1)S(1)} %copy.69), channel_id=1, source_target_pairs={{0,4},{1,5},{2,6},{3,7},{4,0},{5,1},{6,2},{7,3},{8,12},{9,13},{10,... | collective-permute-start | bytes 49160 | tf_op jit(solution)/shard_map/ppermute | solution.py:27
  55.7 4.3 %collective-permute-start.4 = (bf16[64,128]{1,0:T(8,128)(2,1)S(1)}, bf16[64,128]{1,0:T(8,128)(2,1)S(1)}, u32[]{:S(2)}, u32[]{:S(2)}) collective-permute-start(bf16[64,128]{1,0:T(8,128)(2,1)S(1)} %copy.70), channel_id=1, source_target_pairs={{0,5},{1,4},{2,7},{3,6},{4,1},{5,0},{6,3},{7,2},{8,13},{9,12},{10,... | collective-permute-start | bytes 49160 | tf_op jit(solution)/shard_map/ppermute | solution.py:27
  56.1 5.6 %collective-permute-start.5 = (bf16[64,128]{1,0:T(8,128)(2,1)S(1)}, bf16[64,128]{1,0:T(8,128)(2,1)S(1)}, u32[]{:S(2)}, u32[]{:S(2)}) collective-permute-start(bf16[64,128]{1,0:T(8,128)(2,1)S(1)} %copy.71), channel_id=1, source_target_pairs={{0,6},{1,7},{2,4},{3,5},{4,2},{5,3},{6,0},{7,1},{8,14},{9,15},{10,... | collective-permute-start | bytes 49160 | tf_op jit(solution)/shard_map/ppermute | solution.py:27
  59.5 5.0 %collective-permute-start.6 = (bf16[64,128]{1,0:T(8,128)(2,1)S(1)}, bf16[64,128]{1,0:T(8,128)(2,1)S(1)}, u32[]{:S(2)}, u32[]{:S(2)}) collective-permute-start(bf16[64,128]{1,0:T(8,128)(2,1)S(1)} %copy.72), channel_id=1, source_target_pairs={{0,7},{1,6},{2,5},{3,4},{4,3},{5,2},{6,1},{7,0},{8,15},{9,14},{10,... | collective-permute-start | bytes 49160 | tf_op jit(solution)/shard_map/ppermute | solution.py:27
  67.7 1.0 copy-start.1
  67.7 1.1 copy-start.5
  98.0 53.1 %copy-start.10 = (bf16[1,2048,256]{2,1,0:T(8,128)(2,1)S(1)}, bf16[1,2048,256]{2,1,0:T(8,128)(2,1)}, u32[]{:S(2)}) copy-start(bf16[1,2048,256]{2,1,0:T(8,128)(2,1)} %param.36) | copy-start | bytes 3145732
  98.1 116.6 %reduce-scatter.2.cloned.1.call-start = ((), (), s32[]{:S(2)}) async-start(), calls=%async_computation.5 | async-start | bytes 5308416 | tf_op jit(solution)/shard_map/reduce_scatter | solution.py:199
  160.9 59.8 %copy-start.7 = (f32[64,2]{0,1:T(2,128)S(1)}, f32[64,2]{0,1:T(2,128)}, u32[]{:S(2)}) copy-start(f32[64,2]{0,1:T(2,128)} %param.34) | copy-start | bytes 1540
  216.7 11.3 %all-to-all-start.1 = ((bf16[4,36,2048]{2,1,0:T(8,128)(2,1)}), bf16[4,36,2048]{2,1,0:T(8,128)(2,1)S(1)}, u32[]{:S(2)}, u32[]{:S(2)}) async-start(bf16[4,36,2048]{2,1,0:T(8,128)(2,1)} %reshape.245), calls=%async_computation.2 | async-start | bytes 1310720 | tf_op jit(solution)/shard_map/all_to_all | solution.py:205
Sparse Core Ops, SparseCore 0:
  12.3 31.2 all-gather.2
  98.2 47.8 all-gather.4
  161.0 53.6 reduce-scatter.1
